TPU v7x, 128 devices: a 2x2x16 block of a 8x8x16 slice. The times are simulated.
128 devices in a mesh: grp: 4 (over y, x), ep: 32 (over z, core).
Axes of the slice: x: 2, y: 2, z: 16, core: 2. Of those that a mesh axis runs over, the one named last changes fastest.
The devices are a block of a 8x8x16 slice.
Arguments:
- tokens: bfloat16 [4096, 2048], P(('grp', 'ep')), parts along dimension 0, may hold values from -6 to 6
- routes: int32 [4096, 4], P(('grp', 'ep')), parts along dimension 0, may hold values from 0 to 31, all different within a row; in each aligned block of 32 rows (0 to 31, 32 to 63, ...) at most 8 rows name the same one
- route_logits: float32 [4096, 4], P(('grp', 'ep')), parts along dimension 0, may hold values from -4 to 4
- state_real: float32 [4096, 64, 64], P('grp', 'ep'), parts along dimension 0, may hold values from -4 to 4
- state_imag: float32 [4096, 64, 64], P('grp', 'ep'), parts along dimension 0, may hold values from -4 to 4
- gain_in: float32 [2048], replicated, may hold values from 0.1 to 1.9
- proj_in: bfloat16 [2048, 1024], P(None, 'ep'), may hold values from -0.125 to 0.125
- decay_rate: float32 [64, 64], P('ep'), may hold values from 0.05 to 2
- frequency: float32 [64, 64], P('ep'), may hold values from -4 to 4
- log_step: float32 [64], P('ep'), may hold values from -3 to 0
- input_real: float32 [64, 64, 16], P('ep'), may hold values from -1 to 1
- input_imag: float32 [64, 64, 16], P('ep'), may hold values from -1 to 1
- output_real: float32 [64, 16, 64], P('ep'), may hold values from -0.5 to 0.5
- output_imag: float32 [64, 16, 64], P('ep'), may hold values from -0.5 to 0.5
- skip_gain: float32 [64, 16], P('ep'), may hold values from -4 to 4
- proj_out: bfloat16 [1024, 2048], P('ep'), may hold values from -0.1875 to 0.1875
- gain_mid: float32 [2048], replicated, may hold values from 0.1 to 1.9
- expert_gate: bfloat16 [32, 2048, 1024], P('ep'), may hold values from -0.33007812 to 0.33007812
- expert_up: bfloat16 [32, 2048, 1024], P('ep'), may hold values from -0.33007812 to 0.33007812
- expert_down: bfloat16 [32, 1024, 2048], P('ep'), may hold values from -0.056152344 to 0.056152344
- dense_gate: bfloat16 [2048, 2048], P(None, 'ep'), may hold values from -0.125 to 0.125
- dense_up: bfloat16 [2048, 2048], P(None, 'ep'), may hold values from -0.125 to 0.125
- dense_down: bfloat16 [2048, 2048], P('ep'), may hold values from -0.125 to 0.125
- dense_mix: float32 [2048], P('ep'), may hold values from -0.39774758 to 0.39774758
Outputs:
- layer_out: bfloat16 [4096, 2048], P(('grp', 'ep')), parts along dimension 0
- state_real_new: float32 [4096, 64, 64], P('grp', 'ep'), parts along dimension 0
- state_imag_new: float32 [4096, 64, 64], P('grp', 'ep'), parts along dimension 0
There are 4 independent parts, one for each index of `grp`. A program takes and returns all parts, laid end to end along the dimension named above; an argument that names none is the same for every part. Nothing has to cross between parts.
Inputs may be any that keep to these rules, and one draw needn't show every extreme that they name: `routes`: each row names 4 different experts; among the rows of one device no expert is named more than 8 times, and in every draw some device names some expert exactly 8 times.
All inputs are finite; a program needn't handle non-finite values.
Results may differ from a plain program's by a relative error of at most 0.015.
Values may be sent and summed in bfloat16 or wider, within the bound.
A program may use at most 128 MiB of HBM per device.

v0:
```python
import jax
import jax.numpy as jnp
from jax import lax
from jax.sharding import Mesh
from jax.sharding import PartitionSpec as P

EP = ("ep_0", "ep_1")
GRP_EP = ("grp", "ep_0", "ep_1")
EPS = 1e-06
LIMIT = 7.0
ALPHA = 1.702


def copy_for_each(shard, axis):
    length = lax.axis_size(axis)
    return lax.all_to_all(
        jnp.broadcast_to(shard[None], (length, *shard.shape)), axis, 0, 0, tiled=True
    )


def of_everyone(shard, axis):
    return copy_for_each(shard, axis).sum(axis=0)


def reduced_to_own(blocks, axes, turns):
    lengths = [lax.axis_size(a) for a in axes]
    blocks = blocks.reshape(*lengths, *blocks.shape[1:])
    blocks = blocks.transpose(*turns, *range(len(axes), blocks.ndim))
    blocks = blocks.reshape(-1, *blocks.shape[len(axes) :])
    for k in turns:
        blocks = lax.psum_scatter(blocks, axes[k], scatter_dimension=0, tiled=True)
    return blocks[0]


def split_up(shard, dim, length):
    before, after = (shard.shape[:dim], shard.shape[dim + 1 :])
    return jnp.moveaxis(shard.reshape(*before, length, -1, *after), dim, 0)


def scatter_axes(shard, axes, turns, dim):
    length = lax.axis_size(axes)
    return reduced_to_own(split_up(shard, dim, length), axes, turns)


def rms_scale(values, gain_vec):
    return values * lax.rsqrt(jnp.mean(values * values, axis=-1, keepdims=True) + EPS) * gain_vec


def state_step(
    unit_rows,
    state_real,
    state_imag,
    decay_rate,
    frequency,
    log_step,
    input_real,
    input_imag,
    output_real,
    output_imag,
    skip_gain,
):
    seq_count = unit_rows.shape[0]
    groups, group_size = skip_gain.shape
    inputs = unit_rows.astype(jnp.float32).reshape(seq_count, groups, group_size)
    step_size = jnp.exp(log_step)[:, None]
    decay_part = -decay_rate
    magnitude = jnp.exp(decay_part * step_size)
    carry_real = magnitude * jnp.cos(frequency * step_size)
    carry_imag = magnitude * jnp.sin(frequency * step_size)
    denom = decay_part * decay_part + frequency * frequency
    feed_real = ((carry_real - 1.0) * decay_part + carry_imag * frequency) / denom
    feed_imag = (carry_imag * decay_part - (carry_real - 1.0) * frequency) / denom
    drive_real = jnp.einsum("sgp,gnp->sgn", inputs, input_real)
    drive_imag = jnp.einsum("sgp,gnp->sgn", inputs, input_imag)
    new_real = (
        carry_real * state_real
        - carry_imag * state_imag
        + feed_real * drive_real
        - feed_imag * drive_imag
    )
    new_imag = (
        carry_real * state_imag
        + carry_imag * state_real
        + feed_real * drive_imag
        + feed_imag * drive_real
    )
    readout = (
        jnp.einsum("gpn,sgn->sgp", output_real, new_real)
        - jnp.einsum("gpn,sgn->sgp", output_imag, new_imag)
        + skip_gain * inputs
    )
    branch = jax.nn.gelu(readout).reshape(seq_count, groups * group_size).astype(jnp.bfloat16)
    return (branch, new_real, new_imag)


def expert_apply(row_block, gate_weight, up_weight, down_weight):
    gated = jnp.minimum(jnp.dot(row_block, gate_weight, preferred_element_type=jnp.float32), LIMIT)
    upper = jnp.clip(
        jnp.dot(row_block, up_weight, preferred_element_type=jnp.float32), -LIMIT, LIMIT
    )
    activated = ((upper + 1.0) * gated * jax.nn.sigmoid(ALPHA * gated)).astype(jnp.bfloat16)
    return jnp.dot(activated, down_weight, preferred_element_type=jnp.float32).astype(jnp.bfloat16)


def dense_hidden(row_block, dense_gate, dense_up):
    return (
        jax.nn.silu(jnp.dot(row_block, dense_gate, preferred_element_type=jnp.float32))
        * jnp.dot(row_block, dense_up, preferred_element_type=jnp.float32)
    ).astype(jnp.bfloat16)


def on_device(
    tokens,
    routes,
    route_logits,
    state_real,
    state_imag,
    gain_in,
    proj_in,
    decay_rate,
    frequency,
    log_step,
    input_real,
    input_imag,
    output_real,
    output_imag,
    skip_gain,
    proj_out,
    gain_mid,
    expert_gate,
    expert_up,
    expert_down,
    dense_gate,
    dense_up,
    dense_down,
    dense_mix,
):
    devices = lax.axis_size(EP)
    own_rows = tokens.shape[0]
    top_count = routes.shape[1]
    capacity = max(2, 2 * own_rows * top_count // devices)
    inputs = tokens.astype(jnp.float32)
    normed = rms_scale(inputs, gain_in).astype(jnp.bfloat16)
    unit_rows = jnp.dot(
        lax.all_gather(normed, EP, axis=0, tiled=True), proj_in, preferred_element_type=jnp.float32
    ).astype(jnp.bfloat16)
    branch, new_real, new_imag = state_step(
        unit_rows,
        state_real,
        state_imag,
        decay_rate,
        frequency,
        log_step,
        input_real,
        input_imag,
        output_real,
        output_imag,
        skip_gain,
    )
    whole_out = lax.all_gather(proj_out, EP, axis=0, tiled=True)
    own_branch = lax.all_to_all(branch, EP, split_axis=0, concat_axis=1, tiled=True)
    mixer_out = jnp.dot(own_branch, whole_out, preferred_element_type=jnp.float32)
    residual = inputs + mixer_out
    mixed = rms_scale(residual, gain_mid).astype(jnp.bfloat16)
    weights = jnp.exp(route_logits)
    weights = weights / jnp.sum(weights, axis=1, keepdims=True)
    whole_rows = lax.all_gather(mixed, EP, axis=0, tiled=True)
    hidden = dense_hidden(whole_rows, dense_gate, dense_up)
    logit_term = jnp.dot(hidden.astype(jnp.float32), dense_mix)
    expert_ids = jnp.arange(devices, dtype=jnp.int32)
    shares = jnp.sum(
        jnp.where(routes[:, :, None] == expert_ids[None, None, :], weights[:, :, None], 0.0), axis=1
    )
    my_shares = lax.all_to_all(shares, EP, split_axis=1, concat_axis=0, tiled=True)[:, 0]
    gate_logit = of_everyone(logit_term, EP)
    marked = (my_shares > 0.0).astype(jnp.int32)
    rank_rows = jnp.cumsum(marked) - 1
    slot_ids = jnp.arange(devices * capacity, dtype=jnp.int32)
    selector = ((rank_rows[None, :] == slot_ids[:, None]) & (marked[None, :] == 1)).astype(
        jnp.bfloat16
    )
    picked = jnp.dot(selector, whole_rows, preferred_element_type=jnp.float32).astype(jnp.bfloat16)
    result = expert_apply(picked, expert_gate[0], expert_up[0], expert_down[0])
    expert_term = my_shares[:, None] * jnp.dot(
        selector.T, result, preferred_element_type=jnp.float32
    )
    gate_weight = jax.nn.sigmoid(gate_logit)
    dense_part = jnp.dot(hidden, dense_down, preferred_element_type=jnp.float32)
    combined = scatter_axes(
        (gate_weight[:, None] * dense_part + expert_term).astype(jnp.bfloat16), EP, (1, 0), 0
    ).astype(jnp.float32)
    layer_out = (residual + combined).astype(jnp.bfloat16)
    return (layer_out, new_real, new_imag)


def solution(mesh):
    split = Mesh(mesh.devices.reshape(mesh.shape["grp"], 16, 2), ("grp", "ep_0", "ep_1"))
    return jax.shard_map(
        on_device,
        mesh=split,
        in_specs=(
            P(GRP_EP, None),
            P(GRP_EP, None),
            P(GRP_EP, None),
            P("grp", EP, None),
            P("grp", EP, None),
            P(),
            P(None, EP),
            P(EP, None),
            P(EP, None),
            P(EP),
            P(EP, None, None),
            P(EP, None, None),
            P(EP, None, None),
            P(EP, None, None),
            P(EP, None),
            P(EP, None),
            P(),
            P(EP, None, None),
            P(EP, None, None),
            P(EP, None, None),
            P(None, EP),
            P(None, EP),
            P(EP, None),
            P(EP),
        ),
        out_specs=(P(GRP_EP, None), P("grp", EP, None), P("grp", EP, None)),
        check_vma=False,
    )
```

profile of v0, /device:TPU:84, one launch (start us, length us, event | category | flops | bytes accessed | tf_op | source)
XLA Modules:
  0.0 369.5 jit_solution(18087104272636381109)
XLA Ops:
  7.2 0.0 copy-start
  7.2 0.1 all-gather.4.cloned.1.call-start
  7.3 1.1 fusion.39
  8.4 1.7 fusion.41
  10.1 0.1 all-gather.4.cloned.1.call-update
  10.2 0.1 all-gather.6.cloned.1.call-start
  10.2 0.7 all-gather.6.cloned.1.call-update
  11.0 0.1 all-gather.8.cloned.1.call-start
  11.1 0.7 exp.23
  11.7 0.8 cosine_multiply_fusion
  12.6 0.0 copy-start.15
  12.6 74.0 %all-gather.4.cloned.1.call-done = bf16[1024,2048]{1,0:T(8,128)(2,1)} async-done(((bf16[32,2048]{1,0:T(8,128)(2,1)}), bf16[1024,2048]{1,0:T(8,128)(2,1)}) %all-gather.4.cloned.1.call-update) | async-done | bytes 4194320 | tf_op jit(solution)/shard_map/all_gather | solution.py:145
  86.5 3.5 convolution_convert_fusion.1
  90.0 0.0 copy-start.4
  90.1 0.3 fusion.58
  90.4 0.4 bitcast_add_fusion
  90.8 0.0 copy-start.2
  90.8 0.0 copy-start.3
  90.8 0.0 copy-start.12
  90.8 0.2 fusion.59
  91.0 0.2 fusion.50
  91.2 0.2 convert_element_type.63
  91.4 0.3 copy.43
  91.7 0.2 reshape.129
  92.0 23.3 %all_to_all.38 = bf16[32,2,512]{2,1,0:T(2,128)(2,1)S(1)} all-to-all(bf16[32,2,512]{2,1,0:T(2,128)(2,1)S(1)} %reshape.129), channel_id=1, replica_groups=mesh['grp'=4,'ep_0'=16,'ep_1'=2] {'ep_0','ep_1'}, dimensions={0} | all-to-all | bytes 131072 | tf_op jit(solution)/shard_map/all_to_all | solution.py:161
  115.2 0.2 reshape.130
  115.4 0.1 copy.44
  115.5 0.3 all_to_all.30
  115.8 41.1 %all-gather.6.cloned.1.call-done = bf16[1024,2048]{1,0:T(8,128)(2,1)} async-done(((bf16[32,2048]{1,0:T(8,128)(2,1)}), bf16[1024,2048]{1,0:T(8,128)(2,1)}) %all-gather.6.cloned.1.call-update) | async-done | bytes 4194320 | tf_op jit(solution)/shard_map/all_gather | solution.py:160
  156.9 3.1 multiply_reduce_fusion
  160.1 0.7 multiply_convert_fusion
  160.9 0.1 all-gather.8.cloned.1.call-update
  161.0 0.1 select_reduce_fusion
  161.1 0.1 copy.46
  161.1 19.3 %all_to_all.39 = f32[32,32,1]{0,2,1:T(1,128)S(1)} all-to-all(f32[32,32,1]{0,2,1:T(1,128)S(1)} %copy.46), channel_id=1, replica_groups=mesh['grp'=4,'ep_0'=16,'ep_1'=2] {'ep_0','ep_1'}, dimensions={1} | all-to-all | bytes 8192 | tf_op jit(solution)/shard_map/all_to_all | solution.py:174
  180.5 0.1 fusion.51
  180.6 0.1 reshape.109
  180.7 0.1 mul.264
  180.7 0.3 reduce-window.9
  181.0 0.1 slice.7
  181.1 0.1 slice_reduce_fusion
  181.2 0.1 add_bitcast_fusion
  181.3 45.6 %all-gather.8.cloned.1.call-done = bf16[1024,2048]{1,0:T(8,128)(2,1)} async-done(((bf16[32,2048]{1,0:T(8,128)(2,1)}), bf16[1024,2048]{1,0:T(8,128)(2,1)}) %all-gather.8.cloned.1.call-update) | async-done | bytes 4194320 | tf_op jit(solution)/shard_map/all_gather | solution.py:167
  226.9 3.7 %fusion.60 = f32[1024,64]{0,1:T(8,128)S(1)} fusion(bf16[1024,2048]{1,0:T(8,128)(2,1)} %all-gather.8.cloned.1.call-done, bf16[2048,64]{0,1:T(8,128)(2,1)S(1)} %copy-done.7), kind=kOutput, calls=%fused_computation.75 | convolution fusion | flops 268435456 | bytes 4718592 | tf_op jit(solution)/shard_map/dot_general | solution.py:107
  230.7 1.4 fusion.27
  232.1 0.1 fusion.55
  232.2 0.7 broadcast_in_dim.10
  233.0 9.0 %all-to-all-start.1 = ((f32[32,1,1024]{2,1,0:T(1,128)}), f32[32,1,1024]{2,1,0:T(1,128)S(1)}, u32[]{:S(2)}, u32[]{:S(2)}) async-start(f32[32,1,1024]{2,1,0:T(1,128)} %broadcast_in_dim.10), calls=%async_computation.1 | async-start | bytes 262144 | tf_op jit(solution)/shard_map/all_to_all | solution.py:16
  242.0 0.2 reduce-scatter.3.cloned.1.call-start
  242.3 3.6 convolution_convert_fusion
  245.9 1.3 fusion.9
  247.2 0.9 copy-done.18
  248.1 1.4 fusion.24
  249.5 4.5 %fusion.61 = f32[1024,2048]{1,0:T(8,128)} fusion(bf16[1024,64]{0,1:T(8,128)(2,1)S(1)} %fusion.27, bf16[64,2048]{1,0:T(8,128)(2,1)S(1)} %copy-done), kind=kOutput, calls=%fused_computation.76 | convolution fusion | flops 268435456 | bytes 8781824 | tf_op jit(solution)/shard_map/dot_general | solution.py:188
  254.0 4.5 %all-to-all-done.1 = f32[32,1,1024]{2,1,0:T(1,128)S(1)} async-done(((f32[32,1,1024]{2,1,0:T(1,128)}), f32[32,1,1024]{2,1,0:T(1,128)S(1)}, u32[]{:S(2)}, u32[]{:S(2)}) %all-to-all-start.1) | async-done | bytes 131104 | tf_op jit(solution)/shard_map/all_to_all | solution.py:16
  258.5 0.1 reduce_sum.47
  258.6 8.6 %add_convert_fusion = bf16[1024,2048]{1,0:T(8,128)(2,1)} fusion(f32[1024,2048]{1,0:T(8,128)} %fusion.61, f32[1024]{0:T(1024)S(1)} %mul.264, f32[1024]{0:T(1024)S(1)} %add_divide_fusion, bf16[256,1024]{1,0:T(8,128)(2,1)S(1)} %fusion.24, bf16[1,1024,2048]{2,1,0:T(8,128)(2,1)} %param.43, s32[1024]{0:T(1024)S(1)} %add_bitcast_fusion, ...), kind=kOutput, calls=%fused_computation | convolution fusion | flops 2156920832 | bytes 17314816 | tf_op jit(solution)/shard_map/dot_general | solution.py:184
  267.2 4.7 %copy.47 = bf16[16,2,32,2048]{3,2,0,1:T(8,128)(2,1)} copy(bf16[16,2,32,2048]{3,2,1,0:T(8,128)(2,1)} %bitcast.98) | data formatting | bytes 8388608 | tf_op jit(solution)/shard_map/reshape;reshape | solution.py:27
  271.9 0.1 reduce-scatter.3.cloned.1.call-update
  272.0 0.1 reduce-scatter.5.cloned.1.call-start
  272.1 15.7 %reduce-scatter.3.cloned.1.call-done = bf16[16,32,2048]{2,1,0:T(8,128)(2,1)} async-done(((bf16[32,32,2048]{2,1,0:T(8,128)(2,1)}), bf16[16,32,2048]{2,1,0:T(8,128)(2,1)}) %reduce-scatter.3.cloned.1.call-update) | async-done | bytes 2097168 | tf_op jit(solution)/shard_map/reduce_scatter | solution.py:31
  287.7 0.1 reduce-scatter.5.cloned.1.call-update
  287.8 73.6 %reduce-scatter.5.cloned.1.call-done = bf16[1,32,2048]{2,1,0:T(8,128)(2,1)} async-done(((bf16[16,32,2048]{2,1,0:T(8,128)(2,1)}), bf16[1,32,2048]{2,1,0:T(8,128)(2,1)}) %reduce-scatter.5.cloned.1.call-update) | async-done | bytes 131088 | tf_op jit(solution)/shard_map/reduce_scatter | solution.py:31
  361.4 1.6 fusion.42
  (41 shorter events, 0.2 us)
Async XLA Ops:
  7.2 242.3 %copy-start = (bf16[64,2048]{1,0:T(8,128)(2,1)S(1)}, bf16[64,2048]{1,0:T(8,128)(2,1)}, u32[]{:S(2)}) copy-start(bf16[64,2048]{1,0:T(8,128)(2,1)} %param.46) | copy-start | bytes 786436
  7.2 82.9 %copy-start.9 = (f32[2,64,16]{1,2,0:T(8,128)S(1)}, f32[2,64,16]{1,2,0:T(8,128)}, u32[]{:S(2)}) copy-start(f32[2,64,16]{1,2,0:T(8,128)} %param.35) | copy-start | bytes 24580
  7.2 83.1 %copy-start.8 = (f32[2,64,16]{1,2,0:T(8,128)S(1)}, f32[2,64,16]{1,2,0:T(8,128)}, u32[]{:S(2)}) copy-start(f32[2,64,16]{1,2,0:T(8,128)} %param.34) | copy-start | bytes 24580
  7.2 83.1 %copy-start.6 = (f32[1024,2,64]{0,2,1:T(8,128)S(1)}, f32[1024,2,64]{0,2,1:T(8,128)}, u32[]{:S(2)}) copy-start(f32[1024,2,64]{0,2,1:T(8,128)} %param.28) | copy-start | bytes 1572868
  7.2 83.1 %copy-start.5 = (f32[1024,2,64]{0,2,1:T(8,128)S(1)}, f32[1024,2,64]{0,2,1:T(8,128)}, u32[]{:S(2)}) copy-start(f32[1024,2,64]{0,2,1:T(8,128)} %param.27) | copy-start | bytes 1572868
  7.2 79.3 %all-gather.4.cloned.1.call-start = ((), (), s32[]{:S(2)}) async-start(), calls=%async_computation.5 | async-start | bytes 4325376 | tf_op jit(solution)/shard_map/all_gather | solution.py:145
  10.2 146.8 %all-gather.6.cloned.1.call-start = ((), (), s32[]{:S(2)}) async-start(), calls=%async_computation.6 | async-start | bytes 4325376 | tf_op jit(solution)/shard_map/all_gather | solution.py:160
  11.0 215.9 %all-gather.8.cloned.1.call-start = ((), (), s32[]{:S(2)}) async-start(), calls=%async_computation.7 | async-start | bytes 4325376 | tf_op jit(solution)/shard_map/all_gather | solution.py:167
  12.5 78.3 %copy-start.11 = (f32[2,16,64]{2,1,0:T(8,128)S(1)}, f32[2,16,64]{2,1,0:T(8,128)}, u32[]{:S(2)}) copy-start(f32[2,16,64]{2,1,0:T(8,128)} %param.36) | copy-start | bytes 24580
  12.5 78.4 %copy-start.10 = (f32[2,16,64]{2,1,0:T(8,128)S(1)}, f32[2,16,64]{2,1,0:T(8,128)}, u32[]{:S(2)}) copy-start(f32[2,16,64]{2,1,0:T(8,128)} %param.37) | copy-start | bytes 24580
  12.6 78.4 %copy-start.15 = (f32[2,16]{1,0:T(2,128)S(1)}, f32[2,16]{1,0:T(2,128)}, u32[]{:S(2)}) copy-start(f32[2,16]{1,0:T(2,128)} %param.38) | copy-start | bytes 388
  90.0 66.9 %copy-start.4 = (bf16[32,2048]{1,0:T(8,128)(2,1)S(1)}, bf16[32,2048]{1,0:T(8,128)(2,1)}, u32[]{:S(2)}) copy-start(bf16[32,2048]{1,0:T(8,128)(2,1)} %param.24) | copy-start | bytes 393220
  90.8 69.3 %copy-start.2 = (f32[1024,2,64]{0,2,1:T(8,128)}, f32[1024,2,64]{0,2,1:T(8,128)S(1)}, u32[]{:S(2)}) copy-start(f32[1024,2,64]{0,2,1:T(8,128)S(1)} %get-tuple-element.3) | copy-start | bytes 1572868
  90.8 69.3 %copy-start.3 = (f32[1024,2,64]{0,2,1:T(8,128)}, f32[1024,2,64]{0,2,1:T(8,128)S(1)}, u32[]{:S(2)}) copy-start(f32[1024,2,64]{0,2,1:T(8,128)S(1)} %get-tuple-element.4) | copy-start | bytes 1572868
  90.8 69.3 %copy-start.12 = (f32[2048]{0:T(1024)S(1)}, f32[2048]{0:T(1024)}, u32[]{:S(2)}) copy-start(f32[2048]{0:T(1024)} %param.40) | copy-start | bytes 24580
  91.0 69.9 %copy-start.13 = (f32[32,4]{0,1:T(4,128)S(1)}, f32[32,4]{0,1:T(4,128)}, u32[]{:S(2)}) copy-start(f32[32,4]{0,1:T(4,128)} %param.26) | copy-start | bytes 1540
  91.0 70.0 %copy-start.14 = (s32[32,4]{0,1:T(4,128)S(1)}, s32[32,4]{0,1:T(4,128)}, u32[]{:S(2)}) copy-start(s32[32,4]{0,1:T(4,128)} %param.25) | copy-start | bytes 1540
  91.0 135.9 %copy-start.7 = (bf16[2048,64]{0,1:T(8,128)(2,1)S(1)}, bf16[2048,64]{0,1:T(8,128)(2,1)}, u32[]{:S(2)}) copy-start(bf16[2048,64]{0,1:T(8,128)(2,1)} %param.44) | copy-start | bytes 786436
  160.1 70.6 %copy-start.19 = (bf16[2048,64]{0,1:T(8,128)(2,1)S(1)}, bf16[2048,64]{0,1:T(8,128)(2,1)}, u32[]{:S(2)}) copy-start(bf16[2048,64]{0,1:T(8,128)(2,1)} %param.45) | copy-start | bytes 786436
  226.9 3.7 %copy-start.1 = (bf16[1024,2048]{1,0:T(8,128)(2,1)S(1)}, bf16[1024,2048]{1,0:T(8,128)(2,1)}, u32[]{:S(2)}) copy-start(bf16[1024,2048]{1,0:T(8,128)(2,1)} %all-gather.8.cloned.1.call-done) | copy-start | bytes 12582916
  230.7 1.4 copy-start.16
  233.0 25.6 %all-to-all-start.1 = ((f32[32,1,1024]{2,1,0:T(1,128)}), f32[32,1,1024]{2,1,0:T(1,128)S(1)}, u32[]{:S(2)}, u32[]{:S(2)}) async-start(f32[32,1,1024]{2,1,0:T(1,128)} %broadcast_in_dim.10), calls=%async_computation.1 | async-start | bytes 262144 | tf_op jit(solution)/shard_map/all_to_all | solution.py:16
  242.0 45.7 %reduce-scatter.3.cloned.1.call-start = ((), (), s32[]{:S(2)}) async-start(), calls=%async_computation.8 | async-start | bytes 6291456 | tf_op jit(solution)/shard_map/reduce_scatter | solution.py:31
  242.3 3.6 copy-start.17
  245.9 2.2 copy-start.18
  272.0 89.4 %reduce-scatter.5.cloned.1.call-start = ((), (), s32[]{:S(2)}) async-start(), calls=%async_computation.9 | async-start | bytes 2228224 | tf_op jit(solution)/shard_map/reduce_scatter | solution.py:31
Sparse Core Ops, SparseCore 0:
  10.3 76.1 all-gather.3
  88.2 68.6 all-gather.5
  161.0 65.8 all-gather.7
  272.1 15.5 reduce-scatter.2
  290.0 71.3 reduce-scatter.4
where the time goes:
time: 370 us; the launch traced here: 369 us
  waiting for transfers between devices  255 us (69%)
  blocking collectives  42.6 us (12%)
  matrix products  32.3 us (9%)
  between operations  14.2 us (4%)
  starting transfers between devices  9.54 us (3%)
  local copies, waits for them, and re-layouts  8.9 us (2%)
  other arithmetic  6.62 us (2%)
    reduce_scatter x2, waiting for transfers between devices, reduced_to_own(): blocks = lax.psum_scatter(blocks, axes[k], scatter_dimension=0, tiled=True)  89.2 us
    all_gather x1, waiting for transfers between devices, on_device(): lax.all_gather(normed, EP, axis=0, tiled=True)  74 us
    all_gather x1, waiting for transfers between devices, on_device(): whole_rows = lax.all_gather(mixed, EP, axis=0, tiled=True)  45.6 us
    all_gather x1, waiting for transfers between devices, on_device(): whole_out = lax.all_gather(proj_out, EP, axis=0, tiled=True)  41.1 us
    all_to_all x1, blocking collectives, on_device(): lax.all_to_all(branch, EP, split_axis=0, concat_axis=1, tiled=True)  23.3 us
    all_to_all x1, blocking collectives, on_device(): lax.all_to_all(shares, EP, split_axis=1, concat_axis=0, tiled=True)[:, 0]  19.3 us
    all_to_all x1, starting transfers between devices, copy_for_each(): lax.all_to_all(jnp.broadcast_to(shard[None], (length, *shard.shape)), axi...  9.04 us
    dot_general x1, matrix products, on_device(): jnp.dot(selector.T, result, preferred_element_type=jnp.float32)  8.6 us
  transfers between devices with their start and end apart: 6, of which 6 were waited for; matrix products, arithmetic and copies ran while one was open for 5% of the time, Pallas kernels for 0%

commit v1 on v0

--- a/solution.py
+++ b/solution.py
@@ -157,7 +157,9 @@
         output_imag,
         skip_gain,
     )
-    whole_out = lax.all_gather(proj_out, EP, axis=0, tiled=True)
+    whole_out = jnp.concatenate(
+        lax.all_to_all(jnp.stack([proj_out] * lax.axis_size(EP)), EP, 0, 0), axis=0
+    )
     own_branch = lax.all_to_all(branch, EP, split_axis=0, concat_axis=1, tiled=True)
     mixer_out = jnp.dot(own_branch, whole_out, preferred_element_type=jnp.float32)
     residual = inputs + mixer_out

time: 370 us -> 522 us (1.41)
  waiting for transfers between devices: 255 us -> 404 us
  starting transfers between devices: 9.54 us -> 14.9 us
    all_to_all x0 -> x1, waiting for transfers between devices: none -> 190 us  [on_device(): lax.all_to_all(jnp.stack([proj_out] * lax.axis_size(EP)), EP, 0, 0)]
    all_gather x1 -> x0, waiting for transfers between devices: 41.1 us -> none  [on_device(): whole_out = lax.all_gather(proj_out, EP, axis=0, tiled=True)]
    all_to_all x0 -> x1, starting transfers between devices: none -> 5.8 us  [on_device(): lax.all_to_all(jnp.stack([proj_out] * lax.axis_size(EP)), EP, 0, 0)]
  transfers between devices with their start and end apart: 6 -> 6, of which waited for: 6 -> 6; matrix products, arithmetic and copies ran while one was open for 5% -> 3% of each run, Pallas kernels for 0% -> 0%
where the time goes in v1:
time: 522 us; the launch traced here: 521 us
  waiting for transfers between devices  404 us (77%)
  blocking collectives  38.2 us (7%)
  matrix products  32.4 us (6%)
  starting transfers between devices  14.9 us (3%)
  between operations  14.2 us (3%)
  local copies, waits for them, and re-layouts  11 us (2%)
  other arithmetic  6.62 us (1%)
    all_to_all x1, waiting for transfers between devices, on_device(): lax.all_to_all(jnp.stack([proj_out] * lax.axis_size(EP)), EP, 0, 0)  190 us
    reduce_scatter x2, waiting for transfers between devices, reduced_to_own(): blocks = lax.psum_scatter(blocks, axes[k], scatter_dimension=0, tiled=True)  89.1 us
    all_gather x1, waiting for transfers between devices, on_device(): lax.all_gather(normed, EP, axis=0, tiled=True)  74.8 us
    all_gather x1, waiting for transfers between devices, on_device(): whole_rows = lax.all_gather(mixed, EP, axis=0, tiled=True)  45.1 us
    all_to_all x1, blocking collectives, on_device(): lax.all_to_all(branch, EP, split_axis=0, concat_axis=1, tiled=True)  22.6 us
    all_to_all x1, blocking collectives, on_device(): lax.all_to_all(shares, EP, split_axis=1, concat_axis=0, tiled=True)[:, 0]  15.6 us
  transfers between devices with their start and end apart: 6, of which 6 were waited for; matrix products, arithmetic and copies ran while one was open for 3% of the time, Pallas kernels for 0%

profile of v1, /device:TPU:84, one launch (start us, length us, event | category | flops | bytes accessed | tf_op | source)
XLA Modules:
  0.0 521.5 jit_solution(7528500858881764716)
XLA Ops:
  7.2 0.0 copy-start
  7.2 0.1 all-gather.3.cloned.1.call-start
  7.3 1.1 fusion.40
  8.4 1.7 fusion.42
  10.1 0.1 all-gather.3.cloned.1.call-update
  10.2 0.7 exp.23
  10.8 0.8 cosine_multiply_fusion
  11.6 0.0 copy-start.12
  11.7 0.0 copy-start.11
  11.7 74.8 %all-gather.3.cloned.1.call-done = bf16[1024,2048]{1,0:T(8,128)(2,1)} async-done(((bf16[32,2048]{1,0:T(8,128)(2,1)}), bf16[1024,2048]{1,0:T(8,128)(2,1)}) %all-gather.3.cloned.1.call-update) | async-done | bytes 4194320 | tf_op jit(solution)/shard_map/all_gather | solution.py:145
  86.5 3.5 convolution_convert_fusion.1
  90.0 0.0 copy-start.8
  90.1 0.3 fusion.60
  90.4 0.4 bitcast_add_fusion
  90.8 0.0 copy-start.2
  90.8 0.0 copy-start.3
  90.8 0.2 fusion.61
  91.0 0.2 fusion.52
  91.2 0.2 convert_element_type.63
  91.4 0.3 copy.42
  91.7 0.2 reshape.133
  91.9 22.6 %all_to_all.40 = bf16[32,2,512]{2,1,0:T(2,128)(2,1)S(1)} all-to-all(bf16[32,2,512]{2,1,0:T(2,128)(2,1)S(1)} %reshape.133), channel_id=1, replica_groups=mesh['grp'=4,'ep_0'=16,'ep_1'=2] {'ep_0','ep_1'}, dimensions={0} | all-to-all | bytes 131072 | tf_op jit(solution)/shard_map/all_to_all | solution.py:163
  114.5 2.5 stack.2
  117.0 5.8 %all-to-all-start.1 = ((bf16[32,32,2048]{2,1,0:T(8,128)(2,1)}), bf16[32,32,2048]{2,1,0:T(8,128)(2,1)}, u32[]{:S(2)}, u32[]{:S(2)}) async-start(bf16[32,32,2048]{2,1,0:T(8,128)(2,1)} %stack.2), calls=%async_computation.1 | async-start | bytes 8388608 | tf_op jit(solution)/shard_map/all_to_all | solution.py:161
  122.8 0.0 copy-start.13
  122.9 0.0 copy-start.14
  122.9 0.1 all-gather.5.cloned.1.call-start
  123.0 0.2 reshape.134
  123.2 190.3 %all-to-all-done.1 = bf16[32,32,2048]{2,1,0:T(8,128)(2,1)} async-done(((bf16[32,32,2048]{2,1,0:T(8,128)(2,1)}), bf16[32,32,2048]{2,1,0:T(8,128)(2,1)}, u32[]{:S(2)}, u32[]{:S(2)}) %all-to-all-start.1) | async-done | bytes 4194336 | tf_op jit(solution)/shard_map/all_to_all | solution.py:161
  313.5 3.3 multiply_reduce_fusion
  316.8 0.7 multiply_convert_fusion
  317.6 0.1 all-gather.5.cloned.1.call-update
  317.7 0.1 select_reduce_fusion
  317.8 0.1 copy.44
  317.9 15.6 %all_to_all.41 = f32[32,32,1]{0,2,1:T(1,128)S(1)} all-to-all(f32[32,32,1]{0,2,1:T(1,128)S(1)} %copy.44), channel_id=1, replica_groups=mesh['grp'=4,'ep_0'=16,'ep_1'=2] {'ep_0','ep_1'}, dimensions={1} | all-to-all | bytes 8192 | tf_op jit(solution)/shard_map/all_to_all | solution.py:176
  333.5 0.1 fusion.53
  333.6 0.1 reshape.112
  333.7 0.1 mul.264
  333.7 0.3 reduce-window.9
  334.0 0.1 slice.7
  334.1 0.1 slice_reduce_fusion
  334.2 0.1 add_bitcast_fusion
  334.3 45.1 %all-gather.5.cloned.1.call-done = bf16[1024,2048]{1,0:T(8,128)(2,1)} async-done(((bf16[32,2048]{1,0:T(8,128)(2,1)}), bf16[1024,2048]{1,0:T(8,128)(2,1)}) %all-gather.5.cloned.1.call-update) | async-done | bytes 4194320 | tf_op jit(solution)/shard_map/all_gather | solution.py:169
  379.4 3.7 fusion.62
  383.2 1.4 fusion.28
  384.6 0.1 fusion.57
  384.7 0.7 broadcast_in_dim.10
  385.4 8.6 %all-to-all-start.2 = ((f32[32,1,1024]{2,1,0:T(1,128)}), f32[32,1,1024]{2,1,0:T(1,128)S(1)}, u32[]{:S(2)}, u32[]{:S(2)}) async-start(f32[32,1,1024]{2,1,0:T(1,128)} %broadcast_in_dim.10), calls=%async_computation.2 | async-start | bytes 262144 | tf_op jit(solution)/shard_map/all_to_all | solution.py:16
  394.1 0.2 reduce-scatter.3.cloned.1.call-start
  394.3 3.6 convolution_convert_fusion
  398.0 1.3 fusion.10
  399.2 0.9 copy-done.19
  400.1 1.4 fusion.25
  401.6 4.5 fusion.63
  406.1 4.5 all-to-all-done.2
  410.6 0.1 reduce_sum.47
  410.7 8.6 %add_convert_fusion = bf16[1024,2048]{1,0:T(8,128)(2,1)} fusion(f32[1024,2048]{1,0:T(8,128)} %fusion.63, f32[1024]{0:T(1024)S(1)} %mul.264, f32[1024]{0:T(1024)S(1)} %add_divide_fusion, bf16[256,1024]{1,0:T(8,128)(2,1)S(1)} %fusion.25, bf16[1,1024,2048]{2,1,0:T(8,128)(2,1)} %param.43, s32[1024]{0:T(1024)S(1)} %add_bitcast_fusion, ...), kind=kOutput, calls=%fused_computation | convolution fusion | flops 2156920832 | bytes 17314816 | tf_op jit(solution)/shard_map/dot_general | solution.py:186
  419.3 4.7 copy.45
  424.0 0.1 reduce-scatter.3.cloned.1.call-update
  424.0 0.1 reduce-scatter.5.cloned.1.call-start
  424.1 15.6 %reduce-scatter.3.cloned.1.call-done = bf16[16,32,2048]{2,1,0:T(8,128)(2,1)} async-done(((bf16[32,32,2048]{2,1,0:T(8,128)(2,1)}), bf16[16,32,2048]{2,1,0:T(8,128)(2,1)}) %reduce-scatter.3.cloned.1.call-update) | async-done | bytes 2097168 | tf_op jit(solution)/shard_map/reduce_scatter | solution.py:31
  439.7 0.1 reduce-scatter.5.cloned.1.call-update
  439.8 73.5 %reduce-scatter.5.cloned.1.call-done = bf16[1,32,2048]{2,1,0:T(8,128)(2,1)} async-done(((bf16[16,32,2048]{2,1,0:T(8,128)(2,1)}), bf16[1,32,2048]{2,1,0:T(8,128)(2,1)}) %reduce-scatter.5.cloned.1.call-update) | async-done | bytes 131088 | tf_op jit(solution)/shard_map/reduce_scatter | solution.py:31
  513.3 1.6 fusion.43
  (41 shorter events, 0.2 us)
Async XLA Ops:
  7.2 394.4 %copy-start = (bf16[64,2048]{1,0:T(8,128)(2,1)S(1)}, bf16[64,2048]{1,0:T(8,128)(2,1)}, u32[]{:S(2)}) copy-start(bf16[64,2048]{1,0:T(8,128)(2,1)} %param.46) | copy-start | bytes 786436
  7.2 82.9 %copy-start.10 = (f32[2,64,16]{1,2,0:T(8,128)S(1)}, f32[2,64,16]{1,2,0:T(8,128)}, u32[]{:S(2)}) copy-start(f32[2,64,16]{1,2,0:T(8,128)} %param.35) | copy-start | bytes 24580
  7.2 83.1 %copy-start.9 = (f32[2,64,16]{1,2,0:T(8,128)S(1)}, f32[2,64,16]{1,2,0:T(8,128)}, u32[]{:S(2)}) copy-start(f32[2,64,16]{1,2,0:T(8,128)} %param.34) | copy-start | bytes 24580
  7.2 83.1 %copy-start.6 = (f32[1024,2,64]{0,2,1:T(8,128)S(1)}, f32[1024,2,64]{0,2,1:T(8,128)}, u32[]{:S(2)}) copy-start(f32[1024,2,64]{0,2,1:T(8,128)} %param.28) | copy-start | bytes 1572868
  7.2 83.1 %copy-start.5 = (f32[1024,2,64]{0,2,1:T(8,128)S(1)}, f32[1024,2,64]{0,2,1:T(8,128)}, u32[]{:S(2)}) copy-start(f32[1024,2,64]{0,2,1:T(8,128)} %param.27) | copy-start | bytes 1572868
  7.2 79.3 %all-gather.3.cloned.1.call-start = ((), (), s32[]{:S(2)}) async-start(), calls=%async_computation.6 | async-start | bytes 4325376 | tf_op jit(solution)/shard_map/all_gather | solution.py:145
  11.6 79.2 %copy-start.12 = (f32[2,16,64]{2,1,0:T(8,128)S(1)}, f32[2,16,64]{2,1,0:T(8,128)}, u32[]{:S(2)}) copy-start(f32[2,16,64]{2,1,0:T(8,128)} %param.36) | copy-start | bytes 24580
  11.7 79.3 %copy-start.11 = (f32[2,16,64]{2,1,0:T(8,128)S(1)}, f32[2,16,64]{2,1,0:T(8,128)}, u32[]{:S(2)}) copy-start(f32[2,16,64]{2,1,0:T(8,128)} %param.37) | copy-start | bytes 24580
  11.7 79.3 %copy-start.16 = (f32[2,16]{1,0:T(2,128)S(1)}, f32[2,16]{1,0:T(2,128)}, u32[]{:S(2)}) copy-start(f32[2,16]{1,0:T(2,128)} %param.38) | copy-start | bytes 388
  90.0 24.5 %copy-start.8 = (bf16[32,2048]{1,0:T(8,128)(2,1)S(1)}, bf16[32,2048]{1,0:T(8,128)(2,1)}, u32[]{:S(2)}) copy-start(bf16[32,2048]{1,0:T(8,128)(2,1)} %param.39) | copy-start | bytes 393220
  90.8 26.3 %copy-start.2 = (f32[1024,2,64]{0,2,1:T(8,128)}, f32[1024,2,64]{0,2,1:T(8,128)S(1)}, u32[]{:S(2)}) copy-start(f32[1024,2,64]{0,2,1:T(8,128)S(1)} %get-tuple-element.3) | copy-start | bytes 1572868
  90.8 26.3 %copy-start.3 = (f32[1024,2,64]{0,2,1:T(8,128)}, f32[1024,2,64]{0,2,1:T(8,128)S(1)}, u32[]{:S(2)}) copy-start(f32[1024,2,64]{0,2,1:T(8,128)S(1)} %get-tuple-element.4) | copy-start | bytes 1572868
  117.0 196.4 %copy-start.4 = (bf16[32,2048]{1,0:T(8,128)(2,1)S(1)}, bf16[32,2048]{1,0:T(8,128)(2,1)}, u32[]{:S(2)}) copy-start(bf16[32,2048]{1,0:T(8,128)(2,1)} %param.24) | copy-start | bytes 393220
  117.0 196.4 %all-to-all-start.1 = ((bf16[32,32,2048]{2,1,0:T(8,128)(2,1)}), bf16[32,32,2048]{2,1,0:T(8,128)(2,1)}, u32[]{:S(2)}, u32[]{:S(2)}) async-start(bf16[32,32,2048]{2,1,0:T(8,128)(2,1)} %stack.2), calls=%async_computation.1 | async-start | bytes 8388608 | tf_op jit(solution)/shard_map/all_to_all | solution.py:161
  122.8 194.0 %copy-start.13 = (f32[2048]{0:T(1024)S(1)}, f32[2048]{0:T(1024)}, u32[]{:S(2)}) copy-start(f32[2048]{0:T(1024)} %param.40) | copy-start | bytes 24580
  122.9 194.8 %copy-start.14 = (f32[32,4]{0,1:T(4,128)S(1)}, f32[32,4]{0,1:T(4,128)}, u32[]{:S(2)}) copy-start(f32[32,4]{0,1:T(4,128)} %param.26) | copy-start | bytes 1540
  122.9 194.8 %copy-start.15 = (s32[32,4]{0,1:T(4,128)S(1)}, s32[32,4]{0,1:T(4,128)}, u32[]{:S(2)}) copy-start(s32[32,4]{0,1:T(4,128)} %param.25) | copy-start | bytes 1540
  122.9 256.5 %copy-start.7 = (bf16[2048,64]{0,1:T(8,128)(2,1)S(1)}, bf16[2048,64]{0,1:T(8,128)(2,1)}, u32[]{:S(2)}) copy-start(bf16[2048,64]{0,1:T(8,128)(2,1)} %param.44) | copy-start | bytes 786436
  122.9 256.5 %all-gather.5.cloned.1.call-start = ((), (), s32[]{:S(2)}) async-start(), calls=%async_computation.7 | async-start | bytes 4325376 | tf_op jit(solution)/shard_map/all_gather | solution.py:169
  316.8 66.4 %copy-start.20 = (bf16[2048,64]{0,1:T(8,128)(2,1)S(1)}, bf16[2048,64]{0,1:T(8,128)(2,1)}, u32[]{:S(2)}) copy-start(bf16[2048,64]{0,1:T(8,128)(2,1)} %param.45) | copy-start | bytes 786436
  379.4 3.7 copy-start.1
  383.2 1.4 copy-start.17
  385.4 25.1 %all-to-all-start.2 = ((f32[32,1,1024]{2,1,0:T(1,128)}), f32[32,1,1024]{2,1,0:T(1,128)S(1)}, u32[]{:S(2)}, u32[]{:S(2)}) async-start(f32[32,1,1024]{2,1,0:T(1,128)} %broadcast_in_dim.10), calls=%async_computation.2 | async-start | bytes 262144 | tf_op jit(solution)/shard_map/all_to_all | solution.py:16
  394.1 45.6 %reduce-scatter.3.cloned.1.call-start = ((), (), s32[]{:S(2)}) async-start(), calls=%async_computation.8 | async-start | bytes 6291456 | tf_op jit(solution)/shard_map/reduce_scatter | solution.py:31
  394.3 3.6 copy-start.18
  397.9 2.2 copy-start.19
  424.0 89.3 %reduce-scatter.5.cloned.1.call-start = ((), (), s32[]{:S(2)}) async-start(), calls=%async_computation.9 | async-start | bytes 2228224 | tf_op jit(solution)/shard_map/reduce_scatter | solution.py:31
Sparse Core Ops, SparseCore 0:
  10.3 76.1 all-gather.2
  317.7 61.6 all-gather.4
  424.2 15.5 reduce-scatter.2
  442.0 71.2 reduce-scatter.4
